TPU v7x, 32 devices: a whole 2x2x4 slice. The times are simulated.
32 devices in a mesh: sp: 8 (over z, x), tp: 4 (over y, core).
Axes of the slice: x: 2, y: 2, z: 4, core: 2. Of those that a mesh axis runs over, the one named last changes fastest.
Arguments:
- tokens: bfloat16 [2048, 4096], P('sp', 'tp'), may hold values from -6 to 6
- norm_gain: float32 [2, 4096], replicated, may hold values from 0.1 to 1.9
- w_value: bfloat16 [2, 4096, 2048], P(None, 'sp', 'tp'), may hold values from -0.09375 to 0.09375
- w_gate: bfloat16 [2, 4096, 2048], P(None, 'sp', 'tp'), may hold values from -0.09375 to 0.09375
- conv_taps: float32 [2, 31, 2048], P(None, None, 'tp'), may hold values from -3 to 3
- conv_bias: float32 [2, 2048], P(None, 'tp'), may hold values from -3 to 3
- chan_gain: float32 [2, 2048], P(None, 'tp'), may hold values from 0.1 to 1.9
- chan_bias: float32 [2, 2048], P(None, 'tp'), may hold values from -3 to 3
- w_out: bfloat16 [2, 2048, 4096], P(None, 'sp', 'tp'), may hold values from -0.125 to 0.125
Outputs:
- stream: bfloat16 [2048, 4096], P('sp', 'tp')
All inputs are finite; a program needn't handle non-finite values.
Results may differ from a plain program's by a relative error of at most 0.011.
Values may be sent and summed in bfloat16 or wider, within the bound.
A program may use at most 64 MiB of HBM per device.

v0:
```python
import jax
import jax.numpy as jnp
from jax import lax
from jax.sharding import PartitionSpec as P

LAYERS = 2


def passed_along(value, axis, steps):
    count = lax.axis_size(axis)
    first, last = (max(0, -steps), min(count, count - steps))
    return lax.ppermute(value, axis, [(source, source + steps) for source in range(first, last)])


def shards(tokens, norm_gain, w_value, w_gate, conv_taps, conv_bias, chan_gain, chan_bias, w_out):
    stream = tokens
    kernel = conv_taps.shape[1]
    channels_all = conv_taps.shape[2] * lax.axis_size("tp")
    rows_here = tokens.shape[0]
    all_value, all_gate, all_out = (
        lax.all_gather(w_value, "sp", axis=1, tiled=True),
        lax.all_gather(w_gate, "sp", axis=1, tiled=True),
        lax.all_gather(w_out, "sp", axis=1, tiled=True),
    )
    for layer_index in range(LAYERS):
        whole = lax.all_gather(stream, "tp", axis=1, tiled=True)
        widened = whole.astype(jnp.float32)
        scale = lax.rsqrt(jnp.mean(widened * widened, axis=1, keepdims=True) + 1e-06)
        normed = (widened * scale * norm_gain[layer_index][None, :]).astype(jnp.bfloat16)
        value = jnp.dot(normed, all_value[layer_index], preferred_element_type=jnp.float32)
        gate = jnp.dot(normed, all_gate[layer_index], preferred_element_type=jnp.float32)
        gated = (value * jax.nn.sigmoid(gate)).astype(jnp.bfloat16)
        earlier = passed_along(gated[rows_here - kernel + 1 :], "sp", 1)
        extended = jnp.concatenate([earlier, gated], axis=0).astype(jnp.float32)
        taps_here = conv_taps[layer_index]
        convolved = jnp.zeros(gated.shape, jnp.float32) + conv_bias[layer_index][None, :]
        for tap_index in range(kernel):
            convolved = (
                convolved
                + taps_here[tap_index][None, :] * extended[tap_index : tap_index + rows_here]
            )
        sum_first, sum_second = lax.psum(
            (jnp.sum(convolved, axis=1), jnp.sum(convolved * convolved, axis=1)), "tp"
        )
        center = (sum_first / channels_all)[:, None]
        meansq = (sum_second / channels_all)[:, None]
        spread = meansq - center * center
        shaped = (convolved - center) * lax.rsqrt(spread + 1e-05) * chan_gain[layer_index][
            None, :
        ] + chan_bias[layer_index][None, :]
        activated = jax.nn.silu(shaped).astype(jnp.bfloat16)
        all_channels = lax.all_gather(activated, "tp", axis=1, tiled=True)
        update = jnp.dot(all_channels, all_out[layer_index], preferred_element_type=jnp.float32)
        stream = (stream.astype(jnp.float32) + update).astype(jnp.bfloat16)
    return stream


def solution(mesh):
    placed = (
        P("sp", "tp"),
        P(),
        P(None, "sp", "tp"),
        P(None, "sp", "tp"),
        P(None, None, "tp"),
        P(None, "tp"),
        P(None, "tp"),
        P(None, "tp"),
        P(None, "sp", "tp"),
    )
    return jax.shard_map(
        shards, mesh=mesh, in_specs=placed, out_specs=P("sp", "tp"), check_vma=False
    )
```

profile of v0, /device:TPU:0, one launch (start us, length us, event | category | flops | bytes accessed | tf_op | source)
XLA Modules:
  0.0 507.9 jit_solution(4475153728834175335)
XLA Ops:
  6.5 0.7 all-gather.8.cloned.1.call-update
  9.4 0.8 fusion.105
  10.1 0.8 fusion.103
  10.9 0.8 fusion.101
  11.7 0.9 fusion.100
  12.6 0.9 fusion.99
  13.5 0.9 fusion.102
  14.3 19.9 %all-gather.8.cloned.1.call-done = bf16[256,4096]{1,0:T(8,128)(2,1)} async-done(((bf16[256,1024]{1,0:T(8,128)(2,1)}), bf16[256,4096]{1,0:T(8,128)(2,1)}) %all-gather.8.cloned.1.call-update) | async-done | bytes 2097168 | tf_op jit(solution)/shard_map/all_gather | solution.py:26
  34.2 2.1 fusion
  36.3 124.6 %all-gather.12.cloned.1.call-done = bf16[2,4096,512]{2,1,0:T(8,128)(2,1)} async-done(((bf16[2,512,512]{2,1,0:T(8,128)(2,1)}), bf16[2,4096,512]{2,1,0:T(8,128)(2,1)}) %all-gather.12.cloned.1.call-update) | async-done | bytes 8388624 | tf_op jit(solution)/shard_map/all_gather | solution.py:22
  160.9 4.3 fusion.27
  165.2 120.5 %all-gather.10.cloned.1.call-done = bf16[2,4096,512]{2,1,0:T(8,128)(2,1)} async-done(((bf16[2,512,512]{2,1,0:T(8,128)(2,1)}), bf16[2,4096,512]{2,1,0:T(8,128)(2,1)}) %all-gather.10.cloned.1.call-update) | async-done | bytes 8388624 | tf_op jit(solution)/shard_map/all_gather | solution.py:21
  285.7 3.5 fusion.25
  289.2 2.5 collective-permute-start
  291.8 1.6 collective-permute-done
  293.4 2.7 fusion.95
  296.1 6.1 %all-reduce.1 = (f32[256]{0:T(256)S(1)}, f32[256]{0:T(256)S(1)}) all-reduce(f32[256]{0:T(256)S(1)} %get-tuple-element.8, f32[256]{0:T(256)S(1)} %get-tuple-element.7), channel_id=1, replica_groups=mesh['sp'=8,'tp'=4] {'tp'}, use_global_device_ids=true, to_apply=%region_4.0 | all-reduce | flops 512 | bytes 4096 | tf_op jit(solution)/shard_map/psum | solution.py:42
  302.1 1.0 multiply_convert_fusion.1
  303.2 107.3 %all-gather.16.cloned.1.call-done = bf16[2,2048,1024]{2,1,0:T(8,128)(2,1)} async-done(((bf16[2,256,1024]{2,1,0:T(8,128)(2,1)}), bf16[2,2048,1024]{2,1,0:T(8,128)(2,1)}) %all-gather.16.cloned.1.call-update) | async-done | bytes 8388624 | tf_op jit(solution)/shard_map/all_gather | solution.py:23
  410.5 16.3 %all-gather.14.cloned.1.call-done = bf16[256,2048]{1,0:T(8,128)(2,1)} async-done(((bf16[256,512]{1,0:T(8,128)(2,1)}), bf16[256,2048]{1,0:T(8,128)(2,1)}) %all-gather.14.cloned.1.call-update) | async-done | bytes 1048592 | tf_op jit(solution)/shard_map/all_gather | solution.py:52
  426.8 4.6 fusion.15
  431.4 22.7 %all-gather.18.cloned.1.call-done = bf16[256,4096]{1,0:T(8,128)(2,1)} async-done(((bf16[256,1024]{1,0:T(8,128)(2,1)}), bf16[256,4096]{1,0:T(8,128)(2,1)}) %all-gather.18.cloned.1.call-update) | async-done | bytes 2097168 | tf_op jit(solution)/shard_map/all_gather | solution.py:26
  454.1 2.1 fusion.3
  456.2 4.3 fusion.26
  460.6 3.5 fusion.24
  464.1 3.4 collective-permute-start.1
  467.5 0.9 fusion.98
  469.2 2.6 fusion.94
  471.8 5.9 %all-reduce = (f32[256]{0:T(256)S(1)}, f32[256]{0:T(256)S(1)}) all-reduce(f32[256]{0:T(256)S(1)} %get-tuple-element.6, f32[256]{0:T(256)S(1)} %get-tuple-element.5), channel_id=1, replica_groups=mesh['sp'=8,'tp'=4] {'tp'}, use_global_device_ids=true, to_apply=%region_9.10 | all-reduce | flops 512 | bytes 4096 | tf_op jit(solution)/shard_map/psum | solution.py:42
  477.8 1.0 multiply_convert_fusion
  478.8 17.7 %all-gather.20.cloned.1.call-done = bf16[256,2048]{1,0:T(8,128)(2,1)} async-done(((bf16[256,512]{1,0:T(8,128)(2,1)}), bf16[256,2048]{1,0:T(8,128)(2,1)}) %all-gather.20.cloned.1.call-update) | async-done | bytes 1048592 | tf_op jit(solution)/shard_map/all_gather | solution.py:52
  496.5 4.6 fusion.14
  (33 shorter events, 3.1 us)
Async XLA Ops:
  6.5 27.7 %all-gather.8.cloned.1.call-start = ((), (), s32[]{:S(2)}) async-start(), calls=%async_computation | async-start | bytes 2621440 | tf_op jit(solution)/shard_map/all_gather | solution.py:26
  7.3 153.6 %all-gather.12.cloned.1.call-start = ((), (), s32[]{:S(2)}) async-start(), calls=%async_computation.2 | async-start | bytes 9437184 | tf_op jit(solution)/shard_map/all_gather | solution.py:22
  8.0 277.7 %all-gather.10.cloned.1.call-start = ((), (), s32[]{:S(2)}) async-start(), calls=%async_computation.1 | async-start | bytes 9437184 | tf_op jit(solution)/shard_map/all_gather | solution.py:21
  8.7 401.7 %all-gather.16.cloned.1.call-start = ((), (), s32[]{:S(2)}) async-start(), calls=%async_computation.4 | async-start | bytes 9437184 | tf_op jit(solution)/shard_map/all_gather | solution.py:23
  9.3 417.5 %all-gather.14.cloned.1.call-start = ((), (), s32[]{:S(2)}) async-start(), calls=%async_computation.3 | async-start | bytes 1310720 | tf_op jit(solution)/shard_map/all_gather | solution.py:52
  160.9 124.9 %copy-start = (bf16[256,4096]{1,0:T(8,128)(2,1)S(1)}, bf16[256,4096]{1,0:T(8,128)(2,1)}, u32[]{:S(2)}) copy-start(bf16[256,4096]{1,0:T(8,128)(2,1)} %all-gather.8.cloned.1.call-done) | copy-start | bytes 6291460
  165.2 126.5 %copy-start.4 = (f32[2,512]{1,0:T(2,128)S(1)}, f32[2,512]{1,0:T(2,128)}, u32[]{:S(2)}) copy-start(f32[2,512]{1,0:T(2,128)} %param.16) | copy-start | bytes 12292
  289.2 4.1 collective-permute-start
  293.4 133.4 %copy-start.2 = (bf16[256,1024]{1,0:T(8,128)(2,1)S(1)}, bf16[256,1024]{1,0:T(8,128)(2,1)}, u32[]{:S(2)}) copy-start(bf16[256,1024]{1,0:T(8,128)(2,1)} %param.9) | copy-start | bytes 1572868
  303.1 151.0 %all-gather.18.cloned.1.call-start = ((), (), s32[]{:S(2)}) async-start(), calls=%async_computation.5 | async-start | bytes 2621440 | tf_op jit(solution)/shard_map/all_gather | solution.py:26
  431.4 65.1 %all-gather.20.cloned.1.call-start = ((), (), s32[]{:S(2)}) async-start(), calls=%async_computation.6 | async-start | bytes 1310720 | tf_op jit(solution)/shard_map/all_gather | solution.py:52
  456.2 4.4 copy-start.1
  464.1 5.0 collective-permute-start.1
  469.2 27.3 %copy-start.3 = (bf16[256,1024]{1,0:T(8,128)(2,1)S(1)}, bf16[256,1024]{1,0:T(8,128)(2,1)}, u32[]{:S(2)}) copy-start(bf16[256,1024]{1,0:T(8,128)(2,1)} %fusion.15) | copy-start | bytes 1572868
Sparse Core Ops, SparseCore 0:
  8.9 25.2 all-gather.7
  36.4 124.4 all-gather.11
  163.1 122.6 all-gather.9
  287.8 122.6 all-gather.15
  411.9 14.8 all-gather.13
  431.5 22.5 all-gather.17
  478.9 17.5 all-gather.19
where the time goes:
time: 509 us; the launch traced here: 508 us
  waiting for transfers between devices  434 us (85%)
  matrix products  24.8 us (5%)
  between operations  13.7 us (3%)
  blocking collectives  12 us (2%)
  other arithmetic  11.6 us (2%)
  starting transfers between devices  6.09 us (1%)
  local copies, waits for them, and re-layouts  5.94 us (1%)
    all_gather x1, waiting for transfers between devices, shards(): lax.all_gather(w_gate, 'sp', axis=1, tiled=True)  125 us
    all_gather x1, waiting for transfers between devices, shards(): lax.all_gather(w_value, 'sp', axis=1, tiled=True)  120 us
    all_gather x1, waiting for transfers between devices, shards(): lax.all_gather(w_out, 'sp', axis=1, tiled=True)  107 us
    all_gather x2, waiting for transfers between devices, shards(): whole = lax.all_gather(stream, 'tp', axis=1, tiled=True)  42.5 us
    all_gather x2, waiting for transfers between devices, shards(): all_channels = lax.all_gather(activated, 'tp', axis=1, tiled=True)  34 us
    psum x2, blocking collectives, shards(): lax.psum((jnp.sum(convolved, axis=1), jnp.sum(convolved * convolved, axis...  12 us
  transfers between devices with their start and end apart: 9, of which 9 were waited for; matrix products, arithmetic and copies ran while one was open for 4% of the time, Pallas kernels for 0%

commit v1 on v0

--- a/solution.py
+++ b/solution.py
@@ -1,9 +1,14 @@
+import functools
+
 import jax
 import jax.numpy as jnp
 from jax import lax
+from jax.experimental import pallas as pl
+from jax.experimental.pallas import tpu as pltpu
 from jax.sharding import PartitionSpec as P
 
 LAYERS = 2
+MESH = pl.DeviceIdType.MESH
 
 
 def passed_along(value, axis, steps):
@@ -55,6 +60,342 @@
     return stream
 
 
+def ring_index(place, count):
+    side = place // (count // 2)
+    return (1 - side) * 2 * place + side * (2 * (count - 1 - place) + 1)
+
+
+def module_kernel(
+    n, t, kernel, tok, gain, wv, wg, taps, cbias, cgain, chbias, wo, out,
+    whole, normed, vgbuf, obuf, act, halo, ext, gated, vacc, gacc, oacc, conv, stats,
+    w_send, w_recv, t_send, t_recv, h_send, h_recv,
+):
+    layers = wv.shape[0]
+    rows, d_tp = tok.shape
+    d_sp, c_tp = wv.shape[1], wv.shape[2]
+    c_sp = wo.shape[1]
+    half = c_sp // 2
+    reach = n // 2
+    border = halo.shape[1]
+    d_all, c_all = d_tp * t, c_tp * t
+    me, my = lax.axis_index("sp"), lax.axis_index("tp")
+    z, x = me // 2, me % 2
+    pos = z + x * (n - 1 - 2 * z)
+    side_at = (ring_index((pos + 1) % n, n), ring_index((pos + n - 1) % n, n))
+
+    def slot(way, hop):
+        return hop - 1 if way == 0 or hop == reach else reach + hop - 1
+
+    def sent(l, ph, way, hop, c):
+        if ph == 0:
+            own = (wv, wg)[c].at[l]
+            buf = vgbuf.at[l]
+        else:
+            own = wo.at[l, pl.ds(c * half, half)]
+            buf = obuf.at[l]
+        return pltpu.make_async_remote_copy(
+            src_ref=own if hop == 1 else buf.at[slot(way, hop - 1), c],
+            dst_ref=buf.at[slot(way, hop), c],
+            send_sem=w_send.at[l, ph, way, hop - 1, c],
+            recv_sem=w_recv.at[l, ph, way, hop - 1, c],
+            device_id={"sp": side_at[way]},
+            device_id_type=MESH,
+        )
+
+    def pieces(hop):
+        if hop < reach:
+            return [(0, 0), (1, 1), (0, 1), (1, 0)]
+        return [(0, 0), (1, 1)]
+
+    def begin(l, ph):
+        for way, c in pieces(1):
+            sent(l, ph, way, 1, c).start()
+
+    def event(l, ph, hop):
+        for way, c in pieces(hop):
+            sent(l, ph, way, hop, c).wait_recv()
+            if hop < reach and (way, c) in pieces(hop + 1):
+                sent(l, ph, way, hop + 1, c).start()
+
+    def sources(hop):
+        if hop == reach:
+            return [(slot(0, hop), ring_index((pos + n - hop) % n, n))]
+        return [
+            (slot(0, hop), ring_index((pos + n - hop) % n, n)),
+            (slot(1, hop), ring_index((pos + hop) % n, n)),
+        ]
+
+    def spread(kind, l, buf):
+        found = []
+        for d in range(1, t):
+            found.append(
+                pltpu.make_async_remote_copy(
+                    src_ref=buf.at[l, my],
+                    dst_ref=buf.at[l, my],
+                    send_sem=t_send.at[l, kind, d - 1],
+                    recv_sem=t_recv.at[l, kind, d - 1],
+                    device_id={"tp": (my + d) % t},
+                    device_id_type=MESH,
+                )
+            )
+        return found
+
+    def halo_copy(l):
+        return pltpu.make_async_remote_copy(
+            src_ref=gated.at[l, pl.ds(rows - border, border)],
+            dst_ref=halo.at[l],
+            send_sem=h_send.at[l],
+            recv_sem=h_recv.at[l],
+            device_id={"sp": (me + 1) % n},
+            device_id_type=MESH,
+        )
+
+    def add_vg(l, source, v_ref, g_ref, first=False):
+        block = normed[source]
+        v = jnp.dot(block, v_ref[...], preferred_element_type=jnp.float32)
+        g = jnp.dot(block, g_ref[...], preferred_element_type=jnp.float32)
+        if first:
+            vacc[...] = v
+            gacc[...] = g
+        else:
+            vacc[...] += v
+            gacc[...] += g
+
+    def add_o(l, source, weight, first=False):
+        start = source * c_sp
+        block = act[l, start // c_tp, :, pl.ds(pl.multiple_of(start % c_tp, c_sp), c_sp)]
+        o = jnp.dot(block, weight, preferred_element_type=jnp.float32)
+        if first:
+            oacc[...] = o
+        else:
+            oacc[...] += o
+
+    def norm(l):
+        step = 32
+
+        def body(i, _):
+            at = pl.ds(pl.multiple_of(i * step, step), step)
+            total = jnp.zeros((step, 1), jnp.float32)
+            for j in range(t):
+                wide = whole[l, j, at, :].astype(jnp.float32)
+                total = total + jnp.sum(wide * wide, axis=1, keepdims=True)
+            scale = lax.rsqrt(total / d_all + 1e-06)
+            for b in range(n):
+                j, off = (b * d_sp) // d_tp, (b * d_sp) % d_tp
+                wide = whole[l, j, at, off : off + d_sp].astype(jnp.float32)
+                g = gain[l : l + 1, b * d_sp : (b + 1) * d_sp]
+                normed[b, at, :] = (wide * scale * g).astype(jnp.bfloat16)
+            return 0
+
+        lax.fori_loop(0, rows // step, body, 0)
+
+    def gate_up(l):
+        gated[l] = (vacc[...] * jax.nn.sigmoid(gacc[...])).astype(jnp.bfloat16)
+        ext[border:, :] = gated[l].astype(jnp.float32)
+
+    def convolve(l):
+        step = 64
+        lane = 128
+
+        def body(i, _):
+            base = pl.multiple_of(i * step, step)
+            at = pl.ds(base, step)
+            first = jnp.zeros((step, lane), jnp.float32)
+            second = jnp.zeros((step, lane), jnp.float32)
+            for b in range(c_tp // lane):
+                cols = slice(b * lane, (b + 1) * lane)
+                total = jnp.zeros((step, lane), jnp.float32) + cbias[l : l + 1, cols]
+                window = ext[pl.ds(base, step + border), cols]
+                for shift in range(8):
+                    reads = [
+                        (k, border - kernel + 1 + k - shift)
+                        for k in range(kernel)
+                        if (border - kernel + 1 + k) % 8 == shift
+                    ]
+                    if not reads:
+                        continue
+                    top = max(start for _, start in reads) + step
+                    moved = window[shift : shift + top]
+                    for k, start in reads:
+                        total = total + taps[l, k : k + 1, cols] * moved[start : start + step]
+                conv[at, cols] = total
+                first = first + total
+                second = second + total * total
+            which = lax.broadcasted_iota(jnp.int32, (step, lane), 1)
+            stats[l, my, at, :] = jnp.where(
+                which < lane // 2,
+                jnp.sum(first, axis=1, keepdims=True),
+                jnp.sum(second, axis=1, keepdims=True),
+            )
+            return 0
+
+        lax.fori_loop(0, rows // step, body, 0)
+
+    def activate(l):
+        step = 32
+
+        def body(i, _):
+            at = pl.ds(pl.multiple_of(i * step, step), step)
+            both = stats[l, 0, at, :]
+            for j in range(1, t):
+                both = both + stats[l, j, at, :]
+            both = both / c_all
+            center = both[:, 0:1]
+            spread_ = both[:, 64:65] - center * center
+            shaped = (conv[at, :] - center) * lax.rsqrt(spread_ + 1e-05) * cgain[
+                l : l + 1, :
+            ] + chbias[l : l + 1, :]
+            act[l, my, at, :] = (shaped * jax.nn.sigmoid(shaped)).astype(jnp.bfloat16)
+            return 0
+
+        lax.fori_loop(0, rows // step, body, 0)
+
+    begin(0, 0)
+    whole[0, my] = tok[...]
+    for copy in spread(0, 0, whole):
+        copy.start()
+    for l in range(layers):
+        if l == 0:
+            for copy in spread(0, l, whole):
+                copy.wait_recv()
+            norm(l)
+            event(l, 0, 1)
+        else:
+            event(l, 0, 1)
+            for copy in spread(0, l, whole):
+                copy.wait_recv()
+            norm(l)
+        add_vg(l, me, wv.at[l], wg.at[l], first=True)
+        for hop in range(1, reach + 1):
+            if hop > 1:
+                event(l, 0, hop)
+            if hop == reach - 1:
+                begin(l, 1)
+            for at, source in sources(hop):
+                add_vg(l, source, vgbuf.at[l, at, 0], vgbuf.at[l, at, 1])
+        gate_up(l)
+
+        @pl.when(me < n - 1)
+        def _():
+            halo_copy(l).start()
+
+        @pl.when(me > 0)
+        def _():
+            halo_copy(l).wait_recv()
+            ext[0:border, :] = halo[l].astype(jnp.float32)
+
+        @pl.when(me == 0)
+        def _():
+            ext[0:border, :] = jnp.zeros((border, c_tp), jnp.float32)
+
+        convolve(l)
+        for copy in spread(1, l, stats):
+            copy.start()
+        event(l, 1, 1)
+        for copy in spread(1, l, stats):
+            copy.wait_recv()
+        activate(l)
+        for copy in spread(2, l, act):
+            copy.start()
+        event(l, 1, 2)
+        for copy in spread(2, l, act):
+            copy.wait_recv()
+        add_o(l, me, wo[l], first=True)
+        for hop in range(1, reach + 1):
+            if hop > 2:
+                event(l, 1, hop)
+            if hop == reach - 1 and l + 1 < layers:
+                begin(l + 1, 0)
+            for at, source in sources(hop):
+                add_o(l, source, obuf[l, at].reshape(c_sp, d_tp))
+        stream = (whole[l, my].astype(jnp.float32) + oacc[...]).astype(jnp.bfloat16)
+        if l + 1 < layers:
+            whole[l + 1, my] = stream
+            for copy in spread(0, l + 1, whole):
+                copy.start()
+        else:
+            out[...] = stream
+    for l in range(layers):
+        for ph in range(2):
+            for hop in range(1, reach + 1):
+                for way, c in pieces(hop):
+                    sent(l, ph, way, hop, c).wait_send()
+        for kind, buf in enumerate((whole, stats, act)):
+            for copy in spread(kind, l, buf):
+                copy.wait_send()
+
+        @pl.when(me < n - 1)
+        def _():
+            halo_copy(l).wait_send()
+
+
+def fused(tokens, norm_gain, w_value, w_gate, conv_taps, conv_bias, chan_gain, chan_bias, w_out):
+    n, t = lax.axis_size("sp"), lax.axis_size("tp")
+    layers, d_sp, c_tp = w_value.shape
+    rows, d_tp = tokens.shape
+    c_sp = w_out.shape[1]
+    kernel = conv_taps.shape[1]
+    border = -(-(kernel - 1) // 16) * 16
+    reach = n // 2
+    f32, bf16 = jnp.float32, jnp.bfloat16
+    vmem = pl.BlockSpec(memory_space=pltpu.VMEM)
+    return pl.pallas_call(
+        functools.partial(module_kernel, n, t, kernel),
+        out_shape=jax.ShapeDtypeStruct((rows, d_tp), bf16),
+        in_specs=[vmem] * 9,
+        out_specs=vmem,
+        scratch_shapes=[
+            pltpu.VMEM((layers, t, rows, d_tp), bf16),
+            pltpu.VMEM((n, rows, d_sp), bf16),
+            pltpu.VMEM((layers, n - 1, 2, d_sp, c_tp), bf16),
+            pltpu.VMEM((layers, n - 1, 2, c_sp // 2, d_tp), bf16),
+            pltpu.VMEM((layers, t, rows, c_tp), bf16),
+            pltpu.VMEM((layers, border, c_tp), bf16),
+            pltpu.VMEM((border + rows, c_tp), f32),
+            pltpu.VMEM((layers, rows, c_tp), bf16),
+            pltpu.VMEM((rows, c_tp), f32),
+            pltpu.VMEM((rows, c_tp), f32),
+            pltpu.VMEM((rows, d_tp), f32),
+            pltpu.VMEM((rows, c_tp), f32),
+            pltpu.VMEM((layers, t, rows, 128), f32),
+            pltpu.SemaphoreType.DMA((layers, 2, 2, reach, 2)),
+            pltpu.SemaphoreType.DMA((layers, 2, 2, reach, 2)),
+            pltpu.SemaphoreType.DMA((layers, 3, t - 1)),
+            pltpu.SemaphoreType.DMA((layers, 3, t - 1)),
+            pltpu.SemaphoreType.DMA((layers,)),
+            pltpu.SemaphoreType.DMA((layers,)),
+        ],
+        compiler_params=pltpu.CompilerParams(
+            has_side_effects=True, vmem_limit_bytes=60 * 1024 * 1024
+        ),
+    )(tokens, norm_gain, w_value, w_gate, conv_taps, conv_bias, chan_gain, chan_bias, w_out)
+
+
+def fits(n, t, tokens, w_value, conv_taps, w_out):
+    d_sp, c_tp = w_value.shape[1:]
+    rows, d_tp = tokens.shape
+    c_sp = w_out.shape[1]
+    return (
+        n % 2 == 0
+        and n >= 4
+        and t >= 2
+        and d_sp % 128 == 0
+        and d_tp % d_sp == 0
+        and c_sp % 128 == 0
+        and c_tp % c_sp == 0
+        and rows % 64 == 0
+        and conv_taps.shape[1] <= rows
+    )
+
+
+def local(tokens, norm_gain, w_value, w_gate, conv_taps, conv_bias, chan_gain, chan_bias, w_out):
+    args = (tokens, norm_gain, w_value, w_gate, conv_taps, conv_bias, chan_gain, chan_bias, w_out)
+    n, t = lax.axis_size("sp"), lax.axis_size("tp")
+    if fits(n, t, tokens, w_value, conv_taps, w_out):
+        return fused(*args)
+    return shards(*args)
+
+
 def solution(mesh):
     placed = (
         P("sp", "tp"),
@@ -68,5 +409,5 @@
         P(None, "sp", "tp"),
     )
     return jax.shard_map(
-        shards, mesh=mesh, in_specs=placed, out_specs=P("sp", "tp"), check_vma=False
+        local, mesh=mesh, in_specs=placed, out_specs=P("sp", "tp"), check_vma=False
     )

time: 509 us -> 261 us (0.51)
  waiting for transfers between devices: 434 us -> 0 us
  Pallas kernels: 0 us -> 257 us
  matrix products: 24.8 us -> 0 us
  between operations: 13.7 us -> 0.01 us
  blocking collectives: 12 us -> 0 us
  other arithmetic: 11.6 us -> 0 us
  starting transfers between devices: 6.09 us -> 0 us
    all_gather x7 -> x0, waiting for transfers between devices: 429 us -> none  [the longest x1 125 us: shards(): lax.all_gather(w_gate, 'sp', axis=1, tiled=True)]
    pallas_call x0 -> x1, Pallas kernels: none -> 257 us  [fused(): pl.pallas_call(functools.partial(module_kernel, n, t, kernel), out_shape=...]
    dot_general x6 -> x0, matrix products: 24.8 us -> none  [the longest x2 9.13 us: shards(): jnp.dot(all_channels, all_out[layer_index], preferred_element_type=jnp.fl...]
    psum x2 -> x0, blocking collectives: 12 us -> none  [shards(): lax.psum((jnp.sum(convolved, axis=1), jnp.sum(convolved * convolved, axis...]
    reduce_sum x4 -> x0, other arithmetic: 9.46 us -> none  [the longest x2 5.29 us: shards(): jnp.sum(convolved, axis=1)]
    slice x10 -> x0, local copies, waits for them, and re-layouts: 5.91 us -> none  [the longest x4 3.48 us: shards(): taps_here[tap_index][None, :] * extended[tap_index:tap_index + rows_here]]
    ppermute x2 -> x0, starting transfers between devices: 5.86 us -> none  [passed_along(): lax.ppermute(value, axis, [(source, source + steps) for source in range(f...]
  transfers between devices with their start and end apart: 9 -> 0, of which waited for: 9 -> 0; matrix products, arithmetic and copies ran while one was open for 4% -> 0% of each run, Pallas kernels for 0% -> 0%
where the time goes in v1:
time: 261 us; the launch traced here: 260 us
  Pallas kernels  257 us (98%)
  local copies, waits for them, and re-layouts  3.45 us (1%)
    pallas_call x1, Pallas kernels, fused(): pl.pallas_call(functools.partial(module_kernel, n, t, kernel), out_shape=...  257 us

profile of v1, /device:TPU:0, one launch (start us, length us, event | category | flops | bytes accessed | tf_op | source)
XLA Modules:
  0.0 260.3 jit_solution(7912436456462291395)
XLA Ops:
  0.0 1.6 copy.10.taps
  1.6 256.8 %shard_map.91 = bf16[256,1024]{1,0:T(8,128)(2,1)} custom-call(bf16[256,1024]{1,0:T(8,128)(2,1)} %tok.1, f32[2,4096]{1,0:T(2,128)} %gain.1, bf16[2,512,512]{2,1,0:T(8,128)(2,1)} %wv.1, bf16[2,512,512]{2,1,0:T(8,128)(2,1)} %wg.1, f32[2,31,512]{2,1,0:T(8,128)} %copy.10.taps, f32[2,512]{1,0:T(2,128)} %cbias.1, f32[2,512]{1,0:T(2,128)} %cgain.1, ...), custom_call_target="tpu_custom_call" | custom-call | tf_op jit(solution)/shard_map/pallas_call | solution.py:342
  258.4 1.9 copy.12

commit v2 on v1

--- a/solution.py
+++ b/solution.py
@@ -66,9 +66,11 @@
 
 
 def module_kernel(
-    n, t, kernel, tok, gain, wv, wg, taps, cbias, cgain, chbias, wo, out,
+    n, t, kernel, tok, gain, wv_far, wg_far, taps, cbias, cgain, chbias, wo_far, out,
     whole, normed, vgbuf, obuf, act, halo, ext, gated, vacc, gacc, oacc, conv, stats,
+    wv, wg, wo, scaled, blocks, sums_out, sums_in, squares,
     w_send, w_recv, t_send, t_recv, h_send, h_recv,
+    l_sem, a_send, a_recv, s_send, s_recv, r_send, r_recv,
 ):
     layers = wv.shape[0]
     rows, d_tp = tok.shape
@@ -88,10 +90,10 @@
 
     def sent(l, ph, way, hop, c):
         if ph == 0:
-            own = (wv, wg)[c].at[l]
-            buf = vgbuf.at[l]
+            own = (wv_far, wg_far)[c].at[l]
+            buf = vgbuf.at[l - 1]
         else:
-            own = wo.at[l, pl.ds(c * half, half)]
+            own = wo_far.at[l, pl.ds(c * half, half)]
             buf = obuf.at[l]
         return pltpu.make_async_remote_copy(
             src_ref=own if hop == 1 else buf.at[slot(way, hop - 1), c],
@@ -190,7 +192,14 @@
         lax.fori_loop(0, rows // step, body, 0)
 
     def gate_up(l):
-        gated[l] = (vacc[...] * jax.nn.sigmoid(gacc[...])).astype(jnp.bfloat16)
+        value, gate = vacc[...], gacc[...]
+        if l == 0:
+            total = squares[0, 0]
+            for j in range(1, t):
+                total = total + squares[0, j]
+            scale = lax.rsqrt(total[:, 0:1] / d_all + 1e-06)
+            value, gate = value * scale, gate * scale
+        gated[l] = (value * jax.nn.sigmoid(gate)).astype(jnp.bfloat16)
         ext[border:, :] = gated[l].astype(jnp.float32)
 
     def convolve(l):
@@ -250,29 +259,167 @@
 
         lax.fori_loop(0, rows // step, body, 0)
 
-    begin(0, 0)
+    per = d_tp // d_sp
+    part = rows // t
+    mine = pl.ds(pl.multiple_of(my * part, part), part)
+
+    def around(off):
+        return ring_index((pos + off + n) % n, n)
+
+    def local_copies():
+        pairs = ((wv_far, wv), (wg_far, wg), (wo_far, wo))
+        return [pltpu.make_async_copy(a, b, l_sem.at[i]) for i, (a, b) in enumerate(pairs)]
+
+    def deal(u, q):
+        return pltpu.make_async_remote_copy(
+            src_ref=scaled.at[u, pl.ds(q * part, part)],
+            dst_ref=blocks.at[me, pl.ds(q * part, part)],
+            send_sem=a_send.at[u, q],
+            recv_sem=a_recv.at[me],
+            device_id={"sp": my * per + u, "tp": q},
+            device_id_type=MESH,
+        )
+
+    def dealt(source):
+        return pltpu.make_async_remote_copy(
+            src_ref=scaled.at[0, mine],
+            dst_ref=blocks.at[source, mine],
+            send_sem=a_send.at[0, 0],
+            recv_sem=a_recv.at[source],
+            device_id={"sp": source, "tp": my},
+            device_id_type=MESH,
+        )
+
+    def share(source, d):
+        return pltpu.make_async_remote_copy(
+            src_ref=blocks.at[source, mine],
+            dst_ref=blocks.at[source, mine],
+            send_sem=s_send.at[source, d - 1],
+            recv_sem=s_recv.at[source, d - 1],
+            device_id={"tp": (my + d) % t},
+            device_id_type=MESH,
+        )
+
+    def shared(source):
+        for d in range(1, t):
+            pltpu.make_async_remote_copy(
+                src_ref=blocks.at[source, mine],
+                dst_ref=blocks.at[
+                    source, pl.ds(pl.multiple_of(((my + t - d) % t) * part, part), part)
+                ],
+                send_sem=s_send.at[source, d - 1],
+                recv_sem=s_recv.at[source, d - 1],
+                device_id={"tp": (my + d) % t},
+                device_id_type=MESH,
+            ).wait_recv()
+
+    def passed(way, d, c):
+        return pltpu.make_async_remote_copy(
+            src_ref=sums_out.at[way, d - 1, c],
+            dst_ref=sums_in.at[way, d - 1, c],
+            send_sem=r_send.at[way, d - 1, c],
+            recv_sem=r_recv.at[way, d - 1, c],
+            device_id={"sp": side_at[way]},
+            device_id_type=MESH,
+        )
+
+    def travels(way, d, c):
+        return d < reach or (d == reach and c == way)
+
+    def reduce_step(d):
+        for way in range(2):
+            source = around(d if way == 0 else -d)
+            if d < reach or way == 0:
+                shared(source)
+            for c in (way, 1 - way):
+                if not travels(way, d, c):
+                    continue
+                total = jnp.dot(
+                    blocks[source], (wv, wg)[c][0], preferred_element_type=jnp.float32
+                )
+                if d < reach and travels(way, d + 1, c):
+                    passed(way, d + 1, c).wait_recv()
+                    total = total + sums_in[way, d, c].astype(jnp.float32)
+                sums_out[way, d - 1, c] = total.astype(jnp.bfloat16)
+                passed(way, d, c).start()
+
+    def for_dealt(action):
+        for u in range(per):
+            for q in range(t):
+
+                @pl.when(jnp.logical_or(my * per + u != me, my != q))
+                def _():
+                    action(deal(u, q))
+
+    for copy in local_copies():
+        copy.start()
+    at_home = my == me // per
+
+    for u in range(per):
+        scaled[u] = (
+            tok[:, u * d_sp : (u + 1) * d_sp].astype(jnp.float32)
+            * gain[pl.ds(0, 1), pl.ds(pl.multiple_of((my * per + u) * d_sp, d_sp), d_sp)]
+        ).astype(jnp.bfloat16)
+    for_dealt(lambda copy: copy.start())
+
+    @pl.when(at_home)
+    def _():
+        blocks[me, mine] = scaled[me % per, mine]
+
+    begin(0, 1)
+    wide = tok[...].astype(jnp.float32)
+    squares[0, my] = jnp.broadcast_to(
+        jnp.sum(wide * wide, axis=1, keepdims=True), (rows, squares.shape[3])
+    )
+    for copy in spread(3, 0, squares):
+        copy.start()
     whole[0, my] = tok[...]
-    for copy in spread(0, 0, whole):
-        copy.start()
+    order = [reach] + [o for d in range(reach - 1, 0, -1) for o in (d, -d)] + [0]
+    for off in order:
+        source = around(off)
+        if off == 0:
+
+            @pl.when(jnp.logical_not(at_home))
+            def _():
+                dealt(source).wait_recv()
+
+        else:
+            dealt(source).wait_recv()
+        for d in range(1, t):
+            share(source, d).start()
+    event(0, 1, 1)
+    for copy in local_copies():
+        copy.wait()
+    for d in range(reach, 0, -1):
+        reduce_step(d)
+        if d > 1:
+            event(0, 1, reach - d + 2)
+    begin(1, 0)
+    shared(me)
+    for c, acc in enumerate((vacc, gacc)):
+        acc[...] = jnp.dot(blocks[me], (wv, wg)[c][0], preferred_element_type=jnp.float32)
+        for way in range(2):
+            passed(way, 1, c).wait_recv()
+            acc[...] += sums_in[way, 0, c].astype(jnp.float32)
+    for copy in spread(3, 0, squares):
+        copy.wait_recv()
+
     for l in range(layers):
-        if l == 0:
+        if l > 0:
+            if l > 1:
+                event(l, 0, 1)
+                event(l, 0, 2)
             for copy in spread(0, l, whole):
                 copy.wait_recv()
             norm(l)
-            event(l, 0, 1)
-        else:
-            event(l, 0, 1)
-            for copy in spread(0, l, whole):
-                copy.wait_recv()
-            norm(l)
-        add_vg(l, me, wv.at[l], wg.at[l], first=True)
-        for hop in range(1, reach + 1):
-            if hop > 1:
-                event(l, 0, hop)
-            if hop == reach - 1:
-                begin(l, 1)
-            for at, source in sources(hop):
-                add_vg(l, source, vgbuf.at[l, at, 0], vgbuf.at[l, at, 1])
+            add_vg(l, me, wv.at[l], wg.at[l], first=True)
+            for hop in range(1, reach + 1):
+                if hop > 2:
+                    event(l, 0, hop)
+                if hop == max(2, reach - 1):
+                    begin(l, 1)
+                for at, source in sources(hop):
+                    add_vg(l, source, vgbuf.at[l - 1, at, 0], vgbuf.at[l - 1, at, 1])
         gate_up(l)
 
         @pl.when(me < n - 1)
@@ -291,20 +438,24 @@
         convolve(l)
         for copy in spread(1, l, stats):
             copy.start()
-        event(l, 1, 1)
+        if l > 0:
+            event(l, 1, 1)
         for copy in spread(1, l, stats):
             copy.wait_recv()
         activate(l)
         for copy in spread(2, l, act):
             copy.start()
-        event(l, 1, 2)
+        if l > 0:
+            event(l, 1, 2)
+        elif layers > 1:
+            event(1, 0, 1)
         for copy in spread(2, l, act):
             copy.wait_recv()
         add_o(l, me, wo[l], first=True)
         for hop in range(1, reach + 1):
-            if hop > 2:
+            if l > 0 and hop > 2:
                 event(l, 1, hop)
-            if hop == reach - 1 and l + 1 < layers:
+            if l > 0 and hop == max(2, reach - 1) and l + 1 < layers:
                 begin(l + 1, 0)
             for at, source in sources(hop):
                 add_o(l, source, obuf[l, at].reshape(c_sp, d_tp))
@@ -313,14 +464,31 @@
             whole[l + 1, my] = stream
             for copy in spread(0, l + 1, whole):
                 copy.start()
+            if l == 0:
+                event(1, 0, 2)
         else:
             out[...] = stream
+    for_dealt(lambda copy: copy.wait_send())
+    for source in range(n):
+        for d in range(1, t):
+            share(source, d).wait_send()
+    for d in range(1, reach + 1):
+        for way in range(2):
+            for c in range(2):
+                if travels(way, d, c):
+                    passed(way, d, c).wait_send()
+    for copy in spread(3, 0, squares):
+        copy.wait_send()
     for l in range(layers):
         for ph in range(2):
+            if (l, ph) == (0, 0):
+                continue
             for hop in range(1, reach + 1):
                 for way, c in pieces(hop):
                     sent(l, ph, way, hop, c).wait_send()
         for kind, buf in enumerate((whole, stats, act)):
+            if (l, kind) == (0, 0):
+                continue
             for copy in spread(kind, l, buf):
                 copy.wait_send()
 
@@ -339,15 +507,16 @@
     reach = n // 2
     f32, bf16 = jnp.float32, jnp.bfloat16
     vmem = pl.BlockSpec(memory_space=pltpu.VMEM)
+    far = pl.BlockSpec(memory_space=pl.ANY)
     return pl.pallas_call(
         functools.partial(module_kernel, n, t, kernel),
         out_shape=jax.ShapeDtypeStruct((rows, d_tp), bf16),
-        in_specs=[vmem] * 9,
+        in_specs=[vmem, vmem, far, far, vmem, vmem, vmem, vmem, far],
         out_specs=vmem,
         scratch_shapes=[
             pltpu.VMEM((layers, t, rows, d_tp), bf16),
             pltpu.VMEM((n, rows, d_sp), bf16),
-            pltpu.VMEM((layers, n - 1, 2, d_sp, c_tp), bf16),
+            pltpu.VMEM((layers - 1, n - 1, 2, d_sp, c_tp), bf16),
             pltpu.VMEM((layers, n - 1, 2, c_sp // 2, d_tp), bf16),
             pltpu.VMEM((layers, t, rows, c_tp), bf16),
             pltpu.VMEM((layers, border, c_tp), bf16),
@@ -358,12 +527,27 @@
             pltpu.VMEM((rows, d_tp), f32),
             pltpu.VMEM((rows, c_tp), f32),
             pltpu.VMEM((layers, t, rows, 128), f32),
+            pltpu.VMEM((layers, d_sp, c_tp), bf16),
+            pltpu.VMEM((layers, d_sp, c_tp), bf16),
+            pltpu.VMEM((layers, c_sp, d_tp), bf16),
+            pltpu.VMEM((d_tp // d_sp, rows, d_sp), bf16),
+            pltpu.VMEM((n, rows, d_sp), bf16),
+            pltpu.VMEM((2, reach, 2, rows, c_tp), bf16),
+            pltpu.VMEM((2, reach, 2, rows, c_tp), bf16),
+            pltpu.VMEM((1, t, rows, 128), f32),
             pltpu.SemaphoreType.DMA((layers, 2, 2, reach, 2)),
             pltpu.SemaphoreType.DMA((layers, 2, 2, reach, 2)),
-            pltpu.SemaphoreType.DMA((layers, 3, t - 1)),
-            pltpu.SemaphoreType.DMA((layers, 3, t - 1)),
+            pltpu.SemaphoreType.DMA((layers, 4, t - 1)),
+            pltpu.SemaphoreType.DMA((layers, 4, t - 1)),
             pltpu.SemaphoreType.DMA((layers,)),
             pltpu.SemaphoreType.DMA((layers,)),
+            pltpu.SemaphoreType.DMA((3,)),
+            pltpu.SemaphoreType.DMA((d_tp // d_sp, t)),
+            pltpu.SemaphoreType.DMA((n,)),
+            pltpu.SemaphoreType.DMA((n, t - 1)),
+            pltpu.SemaphoreType.DMA((n, t - 1)),
+            pltpu.SemaphoreType.DMA((2, reach, 2)),
+            pltpu.SemaphoreType.DMA((2, reach, 2)),
         ],
         compiler_params=pltpu.CompilerParams(
             has_side_effects=True, vmem_limit_bytes=60 * 1024 * 1024
@@ -384,6 +568,8 @@
         and c_sp % 128 == 0
         and c_tp % c_sp == 0
         and rows % 64 == 0
+        and rows % (16 * t) == 0
+        and w_value.shape[0] >= 2
         and conv_taps.shape[1] <= rows
     )
 

time: 261 us -> 252 us (0.966); the launches traced: 260 us -> 248 us
  Pallas kernels: 257 us -> 245 us
    pallas_call x1, Pallas kernels: 257 us -> 245 us  [fused(): pl.pallas_call(functools.partial(module_kernel, n, t, kernel), out_shape=...]
where the time goes in v2:
time: 252 us; the launch traced here: 248 us
  Pallas kernels  245 us (97%)
  local copies, waits for them, and re-layouts  3.45 us (1%)
    pallas_call x1, Pallas kernels, fused(): pl.pallas_call(functools.partial(module_kernel, n, t, kernel), out_shape=...  245 us

profile of v2, /device:TPU:0, one launch (start us, length us, event | category | flops | bytes accessed | tf_op | source)
XLA Modules:
  0.0 248.2 jit_solution(3441554731876438899)
XLA Ops:
  0.0 1.6 copy.10.taps
  1.6 244.7 %shard_map.91 = bf16[256,1024]{1,0:T(8,128)(2,1)} custom-call(bf16[256,1024]{1,0:T(8,128)(2,1)} %tok.1, f32[2,4096]{1,0:T(2,128)} %gain.1, bf16[2,512,512]{2,1,0:T(8,128)(2,1)} %wv_far.1, bf16[2,512,512]{2,1,0:T(8,128)(2,1)} %wg_far.1, f32[2,31,512]{2,1,0:T(8,128)} %copy.10.taps, f32[2,512]{1,0:T(2,128)} %cbias.1, f32[2,512]{1,0:T(2,128)} %cgain.1, ...), custom_call_target="tpu_custom_call" | custom-call | tf_op jit(solution)/shard_map/pallas_call | solution.py:511
  246.3 1.9 copy.12

commit v3 on v2

--- a/solution.py
+++ b/solution.py
@@ -355,6 +355,28 @@
         copy.start()
     at_home = my == me // per
 
+    def greet(sp, tp):
+        pl.semaphore_signal(
+            barrier, inc=1, device_id={"sp": sp, "tp": tp}, device_id_type=MESH
+        )
+
+    barrier = pltpu.get_barrier_semaphore()
+    for sp in (side_at[0], side_at[1], (me + n - 1) % n):
+        greet(sp, my)
+    for d in range(1, t):
+        greet(me, (my + d) % t)
+    for i in range(1, n):
+        greet((me + i) % n, me // per)
+
+    @pl.when(jnp.logical_not(at_home))
+    def _():
+        greet(me, me // per)
+        pl.semaphore_wait(barrier, 2 + t + n)
+
+    @pl.when(at_home)
+    def _():
+        pl.semaphore_wait(barrier, 1 + t + n)
+
     for u in range(per):
         scaled[u] = (
             tok[:, u * d_sp : (u + 1) * d_sp].astype(jnp.float32)
@@ -440,6 +462,8 @@
             copy.start()
         if l > 0:
             event(l, 1, 1)
+        elif layers > 1:
+            event(1, 0, 1)
         for copy in spread(1, l, stats):
             copy.wait_recv()
         activate(l)
@@ -447,8 +471,6 @@
             copy.start()
         if l > 0:
             event(l, 1, 2)
-        elif layers > 1:
-            event(1, 0, 1)
         for copy in spread(2, l, act):
             copy.wait_recv()
         add_o(l, me, wo[l], first=True)
@@ -550,7 +572,7 @@
             pltpu.SemaphoreType.DMA((2, reach, 2)),
         ],
         compiler_params=pltpu.CompilerParams(
-            has_side_effects=True, vmem_limit_bytes=60 * 1024 * 1024
+            has_side_effects=True, collective_id=0, vmem_limit_bytes=60 * 1024 * 1024
         ),
     )(tokens, norm_gain, w_value, w_gate, conv_taps, conv_bias, chan_gain, chan_bias, w_out)
 

time: 252 us -> 242 us (0.960)
  Pallas kernels: 245 us -> 234 us
    pallas_call x1, Pallas kernels: 245 us -> 234 us  [fused(): pl.pallas_call(functools.partial(module_kernel, n, t, kernel), out_shape=...]
where the time goes in v3:
time: 242 us; the launch traced here: 238 us
  Pallas kernels  234 us (97%)
  local copies, waits for them, and re-layouts  3.45 us (1%)
    pallas_call x1, Pallas kernels, fused(): pl.pallas_call(functools.partial(module_kernel, n, t, kernel), out_shape=...  234 us

profile of v3, /device:TPU:0, one launch (start us, length us, event | category | flops | bytes accessed | tf_op | source)
XLA Modules:
  0.0 237.7 jit_solution(2595235562368249554)
XLA Ops:
  0.0 1.6 copy.10.taps
  1.6 234.2 %shard_map.91 = bf16[256,1024]{1,0:T(8,128)(2,1)} custom-call(bf16[256,1024]{1,0:T(8,128)(2,1)} %tok.1, f32[2,4096]{1,0:T(2,128)} %gain.1, bf16[2,512,512]{2,1,0:T(8,128)(2,1)} %wv_far.1, bf16[2,512,512]{2,1,0:T(8,128)(2,1)} %wg_far.1, f32[2,31,512]{2,1,0:T(8,128)} %copy.10.taps, f32[2,512]{1,0:T(2,128)} %cbias.1, f32[2,512]{1,0:T(2,128)} %cgain.1, ...), custom_call_target="tpu_custom_call" | custom-call | tf_op jit(solution)/shard_map/pallas_call | solution.py:533
  235.8 1.9 copy.12
